TPU v7x, 512 devices: a whole 4x4x16 slice. The times are simulated.
512 devices in a mesh: sp: 64 (over z, y), tp: 8 (over x, core).
Axes of the slice: x: 4, y: 4, z: 16, core: 2. Of those that a mesh axis runs over, the one named last changes fastest.
Arguments:
- tokens: bfloat16 [8192, 2048], P('sp'), may hold values from -6 to 6
- in_gain: bfloat16 [2048], replicated, may hold values from 0.099609375 to 1.8984375
- w_value: bfloat16 [2048, 4096], P('sp', 'tp'), may hold values from -0.125 to 0.125
- w_gate: bfloat16 [2048, 4096], P('sp', 'tp'), may hold values from -0.125 to 0.125
- w_in_key: bfloat16 [2048, 1024], P('sp', 'tp'), may hold values from -0.125 to 0.125
- w_read: bfloat16 [2048, 1024], P('sp', 'tp'), may hold values from -0.125 to 0.125
- w_step_fwd: bfloat16 [2048, 64], P('sp', 'tp'), may hold values from -0.25 to 0.25
- w_step_bwd: bfloat16 [2048, 64], P('sp', 'tp'), may hold values from -0.25 to 0.25
- conv_value: bfloat16 [5, 4096], P(None, 'tp'), may hold values from -2.5 to 2.5
- conv_key: bfloat16 [5, 1024], P(None, 'tp'), may hold values from -2.5 to 2.5
- conv_read: bfloat16 [5, 1024], P(None, 'tp'), may hold values from -2.5 to 2.5
- step_bias: float32 [2, 64], P(None, 'tp'), may hold values from -4 to -2
- rate: float32 [2, 64], P(None, 'tp'), may hold values from 0 to 1, as said below
- norm_gain: bfloat16 [4096], P('tp'), may hold values from 0.099609375 to 1.8984375
- w_out: bfloat16 [4096, 2048], P('tp', 'sp'), may hold values from -0.09375 to 0.09375
Outputs:
- mixed: bfloat16 [8192, 2048], P('sp')
Inputs may be any that keep to these rules, and one draw needn't show every extreme that they name: `rate`: positive decay rates, one per head and direction.
All inputs are finite; a program needn't handle non-finite values.
Results may differ from a plain program's by a relative error of at most 0.018.
Values may be sent and summed in bfloat16 or wider, within the bound.
A program may use at most 128 MiB of HBM per device.

v0:
```python
import jax
import jax.numpy as jnp
from jax import lax
from jax.sharding import Mesh
from jax.sharding import PartitionSpec as P

HEAD_DIM = 64
STATE = 128
KERNEL = 5
BLOCK = 128
SP = ("sp_0", "sp_1")


EPSILON = 1e-05
FULL_PRECISION = lax.Precision.HIGHEST


def filled_with(x, identity):
    return jax.tree.map(
        lambda part, zero: jnp.zeros_like(part) + jnp.asarray(zero, part.dtype), x, identity
    )


def entering_2(x, axes, combine, identity):
    before = start = filled_with(x, identity)
    total = x
    for axis in reversed(axes):
        length, place = (lax.axis_size(axis), lax.axis_index(axis))
        pieces = jax.tree.map(lambda part: lax.all_gather(part, axis), total)
        inside, total = (start, start)
        for k in reversed(range(length)):
            passed = k > place
            total = combine(total, jax.tree.map(lambda part: part[k], pieces))
            inside = jax.tree.map(lambda new, old: jnp.where(passed, new, old), total, inside)
        before = combine(inside, before)
    return before


def prefix_by_axis(x, axes, combine, identity):
    before = start = filled_with(x, identity)
    total = x
    for axis in reversed(axes):
        length, place = (lax.axis_size(axis), lax.axis_index(axis))
        pieces = jax.tree.map(
            lambda part, kind: lax.all_gather(part.astype(kind), axis),
            total,
            (jnp.bfloat16, jnp.bfloat16),
        )
        inside, total = (start, start)
        for k in range(length):
            passed = k < place
            total = combine(
                total, jax.tree.map(lambda part, own: part[k].astype(own.dtype), pieces, x)
            )
            inside = jax.tree.map(lambda new, old: jnp.where(passed, new, old), total, inside)
        before = combine(inside, before)
    return before


def sent_together(arrays, axis, dim, along):
    widths = [a.shape[along] for a in arrays]
    both = jnp.concatenate(arrays, axis=along)
    out = lax.all_gather(both, axis, axis=dim, tiled=True)
    return tuple(jnp.split(out, [sum(widths[:k]) for k in range(1, len(widths))], axis=along))


def with_halo(cells, sides, width):
    for axis, dim in sides:
        count = lax.axis_size(axis)
        ends = count - 1
        head = lax.slice_in_dim(cells, 0, width, axis=dim)
        tail = lax.slice_in_dim(cells, cells.shape[dim] - width, cells.shape[dim], axis=dim)
        cells = jnp.concatenate(
            [
                lax.ppermute(tail, axis, [(i, (i + 1) % count) for i in range(ends)]),
                cells,
                lax.ppermute(head, axis, [((i + 1) % count, i) for i in range(ends)]),
            ],
            axis=dim,
        )
    return cells


def whole_of(x, axes, dim):
    out = x
    for number in range(len(axes) - 1, -1, -1):
        out = lax.all_gather(out, axes[number], axis=dim, tiled=True)
    return out


def in_blocks(x, dim, length):
    before, after = (x.shape[:dim], x.shape[dim + 1 :])
    return jnp.moveaxis(x.reshape(*before, length, -1, *after), dim, 0)


def sent_and_summed(x, axis, dim):
    length = lax.axis_size(axis)
    parts = lax.all_to_all(in_blocks(x, dim, length), axis, 0, 0, tiled=True)
    return jnp.sum(parts.astype(jnp.float32), axis=0)


def joined_along(parts, dim):
    shape = list(parts.shape[1:])
    shape[dim] *= parts.shape[0]
    return jnp.moveaxis(parts, 0, dim).reshape(shape)


def copy_for_each(x, axis):
    copies = jnp.broadcast_to(x, (lax.axis_size(axis), *x.shape))
    return lax.all_to_all(copies, axis, split_axis=0, concat_axis=0, tiled=True)


def collect(x, axis, dim):
    return joined_along(copy_for_each(x, axis), dim)


def normalize(tensor, gain):
    return tensor * lax.rsqrt(jnp.mean(tensor * tensor, -1, keepdims=True) + EPSILON) * gain


def block_parts(values, step_size, log_decay, in_keys):
    per_group = values.shape[1] // in_keys.shape[1]
    cumulative = jnp.cumsum(log_decay, axis=0)
    log_total = cumulative[-1]
    weighting = jnp.exp(log_total[None, :] - cumulative) * step_size
    key_heads = jnp.repeat(in_keys, per_group, axis=1)
    scaled = (values.astype(jnp.float32) * weighting[:, :, None]).astype(jnp.bfloat16)
    injected = jnp.einsum("jhn,jhp->hpn", key_heads, scaled, preferred_element_type=jnp.float32)
    return (cumulative, jnp.exp(log_total), injected)


def block_step(memory, inputs):
    values, step_size, cumulative, damping, injected, in_keys, read_in = inputs
    per_group = values.shape[1] // in_keys.shape[1]
    scores = jnp.einsum("ign,jgn->ijg", read_in, in_keys, preferred_element_type=jnp.float32)
    scores = jnp.repeat(scores, per_group, axis=2)
    length = values.shape[0]
    below_mask = (jnp.arange(length)[:, None] >= jnp.arange(length)[None, :])[:, :, None]
    gaps = jnp.where(below_mask, cumulative[:, None, :] - cumulative[None, :, :], -jnp.inf)
    weights = (scores * jnp.exp(gaps) * step_size[None, :, :]).astype(jnp.bfloat16)
    within = jnp.einsum("ijh,jhp->ihp", weights, values, preferred_element_type=jnp.float32)
    read_heads = jnp.repeat(read_in.astype(jnp.float32), per_group, axis=1)
    carried = (
        jnp.einsum("ihn,hpn->ihp", read_heads, memory, precision=FULL_PRECISION)
        * jnp.exp(cumulative)[:, :, None]
    )
    memory = damping[:, None, None] * memory + injected
    return (memory, within + carried)


def blocked(tensor):
    blocks = tensor.shape[0] // BLOCK
    return tensor.reshape((blocks, BLOCK) + tensor.shape[1:])


def sweep(block_inputs, memory):
    memory, swept = lax.scan(block_step, memory, block_inputs)
    return (swept.reshape((swept.shape[0] * swept.shape[1],) + swept.shape[2:]), memory)


def settle(damping_blocks, injected_blocks, memory):

    def advance(memory, inputs):
        return (inputs[0][:, None, None] * memory + inputs[1], None)

    memory, unused = lax.scan(advance, memory, (damping_blocks, injected_blocks))
    return memory


def chain(before_pair, after_pair):
    return (
        before_pair[0] * after_pair[0],
        after_pair[0][:, None, None] * before_pair[1] + after_pair[1],
    )


def entering(damping, final_state, backward):
    identity_pair = (jnp.ones_like(damping), jnp.zeros_like(final_state))
    if backward:
        arrived = entering_2((damping, final_state), SP, chain, identity_pair)
    else:
        arrived = prefix_by_axis((damping, final_state), SP, chain, identity_pair)
    return arrived[1]


def body(
    tokens,
    in_gain,
    w_value,
    w_gate,
    w_in_key,
    w_read,
    w_step_fwd,
    w_step_bwd,
    conv_value,
    conv_key,
    conv_read,
    step_bias,
    rate,
    norm_gain,
    w_out,
):
    normed = normalize(tokens.astype(jnp.float32), in_gain.astype(jnp.float32)).astype(jnp.bfloat16)
    weights = sent_together((w_value, w_gate, w_in_key, w_read, w_step_fwd, w_step_bwd), SP, 0, 1)
    projected = [
        jnp.dot(normed, weight, preferred_element_type=jnp.float32).astype(jnp.bfloat16)
        for weight in weights
    ]
    value_raw, gate_raw, key_raw, read_raw, pre_fwd, pre_bwd = projected
    value_cols = value_raw.shape[1]
    key_cols = key_raw.shape[1]
    joined = jnp.concatenate([value_raw, key_raw, read_raw], axis=1)
    padded = with_halo(joined, ((SP, 0),), (KERNEL - 1) // 2)
    kernel_taps = jnp.concatenate([conv_value, conv_key, conv_read], axis=1).astype(jnp.float32)
    length = joined.shape[0]
    summed = jnp.zeros(joined.shape, jnp.float32)
    for offset in range(KERNEL):
        summed = summed + padded[offset : offset + length].astype(jnp.float32) * kernel_taps[offset]
    mixed_in = jax.nn.silu(summed).astype(jnp.bfloat16)
    head_count = value_cols // HEAD_DIM
    group_count = key_cols // STATE
    values = mixed_in[:, :value_cols].reshape(length, head_count, HEAD_DIM)
    in_keys = mixed_in[:, value_cols : value_cols + key_cols].reshape(length, group_count, STATE)
    read_in = mixed_in[:, value_cols + key_cols :].reshape(length, group_count, STATE)
    blank = jnp.zeros((head_count, HEAD_DIM, STATE), jnp.float32)
    summed_heads = jnp.zeros(values.shape, jnp.float32)
    for direction, step_pre in ((0, pre_fwd), (1, pre_bwd)):
        step_size = jax.nn.softplus(step_pre.astype(jnp.float32) + step_bias[direction])
        log_decay = -rate[direction] * step_size
        ordered = (values, step_size, log_decay, in_keys, read_in)
        if direction == 1:
            ordered = tuple((tensor[::-1] for tensor in ordered))
        value_blocks, step_blocks, decay_blocks, key_blocks, read_blocks = [
            blocked(tensor) for tensor in ordered
        ]
        cumulative_blocks, damping_blocks, injected_blocks = jax.vmap(block_parts)(
            value_blocks, step_blocks, decay_blocks, key_blocks
        )
        block_inputs = (
            value_blocks,
            step_blocks,
            cumulative_blocks,
            damping_blocks,
            injected_blocks,
            key_blocks,
            read_blocks,
        )
        damping = jnp.exp(jnp.sum(ordered[2], axis=0))
        final_state = settle(damping_blocks, injected_blocks, blank)
        arriving = entering(damping, final_state, direction == 1)
        swept, final_state = sweep(block_inputs, arriving)
        if direction == 1:
            swept = swept[::-1]
        summed_heads = summed_heads + swept
    gated_out = summed_heads * jax.nn.silu(gate_raw.astype(jnp.float32)).reshape(values.shape)
    head_gain = norm_gain.astype(jnp.float32).reshape(head_count, HEAD_DIM)
    normed_heads = normalize(gated_out, head_gain).astype(jnp.bfloat16).reshape(length, value_cols)
    out_whole = whole_of(w_out, SP, 1)
    own_rows = sent_and_summed(
        jnp.dot(normed_heads, out_whole, preferred_element_type=jnp.float32).astype(jnp.bfloat16),
        "tp",
        0,
    ).astype(jnp.bfloat16)
    return collect(own_rows, "tp", 0)


def solution(mesh):
    split = Mesh(mesh.devices.reshape(16, 4, mesh.shape["tp"]), ("sp_0", "sp_1", "tp"))
    in_specs = (
        P(SP, None),
        P(),
        P(SP, "tp"),
        P(SP, "tp"),
        P(SP, "tp"),
        P(SP, "tp"),
        P(SP, "tp"),
        P(SP, "tp"),
        P(None, "tp"),
        P(None, "tp"),
        P(None, "tp"),
        P(None, "tp"),
        P(None, "tp"),
        P("tp"),
        P("tp", SP),
    )
    out_specs = P(SP, None)
    return jax.shard_map(body, mesh=split, in_specs=in_specs, out_specs=out_specs, check_vma=False)
```

profile of v0, /device:TPU:1, one launch (start us, length us, event | category | flops | bytes accessed | tf_op | source)
XLA Modules:
  0.0 480.4 jit_solution(13676739252099169719)
XLA Ops:
  6.5 0.8 copy.45
  7.4 0.8 copy.46
  8.1 1.5 concatenate.18
  9.7 0.7 convert_element_type.490
  10.4 1.3 dynamic-slice.5
  12.4 1.0 convert_reduce_fusion.3
  13.4 1.2 fusion.23
  14.6 0.8 slice_bitcast_fusion.81
  15.4 141.7 %all-gather.12.cloned.1.call-done = bf16[2048,1296]{1,0:T(8,128)(2,1)} async-done(((bf16[32,1296]{1,0:T(8,128)(2,1)}), bf16[2048,1296]{1,0:T(8,128)(2,1)}) %all-gather.12.cloned.1.call-update) | async-done | bytes 5308432 | tf_op jit(solution)/shard_map/all_gather | solution.py:63
  157.1 1.8 broadcast_multiply_fusion
  158.9 0.1 rev.15
  159.0 0.1 copy.54
  159.1 0.2 reduce_window_sum.18
  159.3 0.1 rev.16
  159.4 1.6 convolution_convert_fusion.1
  161.0 1.6 convolution_convert_fusion.2
  162.5 2.1 fusion.10
  164.7 1.3 collective-permute-start
  166.0 1.3 collective-permute-start.1
  167.3 1.4 compare_select_fusion.1
  168.7 0.2 multiply_bitcast_fusion
  169.0 0.2 dynamic-update-slice
  169.2 10.4 %all-reduce = bf16[32]{0:T(256)(128)(2,1)S(1)} all-reduce(bf16[32]{0:T(256)(128)(2,1)S(1)} %dynamic-update-slice), channel_id=2, replica_groups=mesh['sp_0'=16,'sp_1'=4,'tp'=8] {'sp_1'}, use_global_device_ids=true, to_apply=%add | all-reduce | flops 32 | bytes 128
  179.7 0.3 multiply_convert_fusion.2
  180.1 0.1 copy.49
  180.3 0.1 rev.14
  180.4 0.9 convolution_add_fusion
  181.4 0.1 slice_convert_fusion.1
  181.4 0.1 copy.51
  181.5 0.2 reduce_window_sum.17
  181.8 0.1 broadcast_select_fusion.7
  182.0 0.2 fusion.9
  182.2 9.9 %all-gather.1 = bf16[32,64,128]{2,1,0:T(8,128)(2,1)S(1)} all-gather(bf16[8,64,128]{2,1,0:T(8,128)(2,1)S(1)} %fusion.9), channel_id=3, replica_groups=mesh['sp_0'=16,'sp_1'=4,'tp'=8] {'sp_1'}, dimensions={0}, use_global_device_ids=true | all-gather | bytes 655360 | tf_op jit(solution)/shard_map/all_gather | solution.py:45
  192.1 0.9 fusion.44
  193.0 0.1 reduce_sum.50
  193.1 0.1 exponential_dynamic-update-slice_fusion
  193.2 6.5 %all-reduce.1 = f32[32]{0:T(128)S(1)} all-reduce(f32[32]{0:T(128)S(1)} %exponential_dynamic-update-slice_fusion), channel_id=4, replica_groups=mesh['sp_0'=16,'sp_1'=4,'tp'=8] {'sp_1'}, use_global_device_ids=true, to_apply=%add.1 | all-reduce | flops 32 | bytes 256
  199.7 0.1 broadcast_select_fusion.3
  199.8 18.9 %all-gather.20.cloned.1.call-done = f32[32,64,128]{2,1,0:T(8,128)} async-done(((f32[8,64,128]{2,1,0:T(8,128)}), f32[32,64,128]{2,1,0:T(8,128)}) %all-gather.20.cloned.1.call-update) | async-done | bytes 1048592 | tf_op jit(solution)/shard_map/all_gather | solution.py:29
  218.6 2.0 bitcast_add_fusion
  220.7 9.8 %all_gather.50 = bf16[512,128]{0,1:T(8,128)(2,1)} all-gather(bf16[512,32]{0,1:T(8,128)(2,1)S(1)} %copy-done.1), channel_id=1, replica_groups=mesh['sp_0'=16,'sp_1'=4,'tp'=8] {'sp_1'}, dimensions={1}, use_global_device_ids=true | all-gather | bytes 163840 | tf_op jit(solution)/shard_map/all_gather | solution.py:87
  230.7 2.1 divide_multiply_fusion
  232.9 0.1 copy.57
  233.0 24.4 %all-gather.4 = bf16[16,1,8]{2,1,0:T(2,128)(2,1)S(1)} all-gather(bf16[1,1,8]{2,1,0:T(2,128)(2,1)S(1)} %bitcast.454), channel_id=1, replica_groups=mesh['sp_0'=16,'sp_1'=4,'tp'=8] {'sp_0'}, dimensions={0}, use_global_device_ids=true | all-gather | bytes 272 | tf_op jit(solution)/shard_map/all_gather | solution.py:45
  257.4 21.9 %all-gather.5 = f32[16,1,8]{2,1,0:T(1,128)S(1)} all-gather(f32[1,1,8]{2,1,0:T(1,128)S(1)} %get-tuple-element.150), channel_id=1, replica_groups=mesh['sp_0'=16,'sp_1'=4,'tp'=8] {'sp_0'}, dimensions={0}, use_global_device_ids=true | all-gather | bytes 544 | tf_op jit(solution)/shard_map/all_gather | solution.py:29
  279.4 0.1 convolution_bitcast_fusion.5
  279.5 0.1 copy.50
  279.7 0.1 convolution_bitcast_fusion.4
  279.8 0.1 copy.53
  279.9 6.5 %all-gather.14.cloned.1.call-done = bf16[16,8,64,128]{3,2,1,0:T(8,128)(2,1)} async-done(((bf16[1,8,64,128]{3,2,1,0:T(8,128)(2,1)}), bf16[16,8,64,128]{3,2,1,0:T(8,128)(2,1)}) %all-gather.14.cloned.1.call-update) | async-done | bytes 2097168 | tf_op jit(solution)/shard_map/all_gather | solution.py:45
  286.4 3.4 fusion.6
  289.9 74.2 %all-gather.16.cloned.1.call-done = f32[16,8,64,128]{3,2,1,0:T(8,128)} async-done(((f32[1,8,64,128]{3,2,1,0:T(8,128)}), f32[16,8,64,128]{3,2,1,0:T(8,128)}) %all-gather.16.cloned.1.call-update) | async-done | bytes 4194320 | tf_op jit(solution)/shard_map/all_gather | solution.py:29
  364.0 4.1 fusion.4
  368.1 0.4 fusion.5
  368.5 0.1 rev.17
  368.6 0.4 multiply_reduce_fusion
  369.0 0.1 copy.56
  369.2 0.1 copy.58
  369.4 65.2 %all-gather.18.cloned.1.call-done = bf16[512,2048]{0,1:T(8,128)(2,1)} async-done(((bf16[512,128]{0,1:T(8,128)(2,1)}), bf16[512,2048]{0,1:T(8,128)(2,1)}) %all-gather.18.cloned.1.call-update) | async-done | bytes 2097168 | tf_op jit(solution)/shard_map/all_gather | solution.py:87
  434.6 2.4 convolution_convert_fusion
  437.0 23.2 %all_to_all.10 = bf16[8,16,2048]{2,1,0:T(8,128)(2,1)S(1)} all-to-all(bf16[8,16,2048]{2,1,0:T(8,128)(2,1)S(1)} %bitcast.445), channel_id=1, replica_groups=mesh['sp_0'=16,'sp_1'=4,'tp'=8] {'tp'}, dimensions={0} | all-to-all | bytes 1048576 | tf_op jit(solution)/shard_map/all_to_all | solution.py:98
  460.2 0.1 reduce_sum.52
  460.4 12.8 %all_to_all.11 = bf16[8,16,2048]{2,1,0:T(8,128)(2,1)S(1)} all-to-all(bf16[8,16,2048]{2,1,0:T(8,128)(2,1)S(1)} %broadcast_in_dim.65), channel_id=1, replica_groups=mesh['sp_0'=16,'sp_1'=4,'tp'=8] {'tp'}, dimensions={0} | all-to-all | bytes 1048576 | tf_op jit(solution)/shard_map/all_to_all | solution.py:110
  473.1 0.8 copy.64
  (46 shorter events, 0.9 us)
Async XLA Ops:
  6.5 156.0 %copy-start = (bf16[128,2048]{1,0:T(8,128)(2,1)S(1)}, bf16[128,2048]{1,0:T(8,128)(2,1)}, u32[]{:S(2)}) copy-start(bf16[128,2048]{1,0:T(8,128)(2,1)} %param.15) | copy-start | bytes 1572868
  6.5 150.6 %all-gather.12.cloned.1.call-start = ((), (), s32[]{:S(2)}) async-start(), calls=%async_computation.2 | async-start | bytes 5857280 | tf_op jit(solution)/shard_map/all_gather | solution.py:63
  9.7 209.0 %all-gather.20.cloned.1.call-start = ((), (), s32[]{:S(2)}) async-start(), calls=%async_computation.6 | async-start | bytes 1310720 | tf_op jit(solution)/shard_map/all_gather | solution.py:29
  164.7 15.0 %collective-permute-start = (bf16[2,768]{1,0:T(2,128)(2,1)S(1)}, bf16[2,768]{1,0:T(2,128)(2,1)S(1)}, u32[]{:S(2)}, u32[]{:S(2)}) collective-permute-start(bf16[2,768]{1,0:T(2,128)(2,1)S(1)} %get-tuple-element.79), channel_id=1, source_target_pairs={{0,8},{8,16},{16,24},{24,32},{32,40},{40,48},{48,56},{56,64},{64,7... | collective-permute-start | bytes 9224 | tf_op jit(solution)/shard_map/ppermute | solution.py:75
  166.0 13.7 %collective-permute-start.1 = (bf16[2,768]{1,0:T(2,128)(2,1)S(1)}, bf16[2,768]{1,0:T(2,128)(2,1)S(1)}, u32[]{:S(2)}, u32[]{:S(2)}) collective-permute-start(bf16[2,768]{1,0:T(2,128)(2,1)S(1)} %get-tuple-element.80), channel_id=1, source_target_pairs={{8,0},{16,8},{24,16},{32,24},{40,32},{48,40},{56,48},{64,56},{72,6... | collective-permute-start | bytes 9224 | tf_op jit(solution)/shard_map/ppermute | solution.py:77
  167.3 53.4 %copy-start.1 = (bf16[512,32]{0,1:T(8,128)(2,1)S(1)}, bf16[512,32]{0,1:T(8,128)(2,1)}, u32[]{:S(2)}) copy-start(bf16[512,32]{0,1:T(8,128)(2,1)} %param.29) | copy-start | bytes 98308
  167.3 63.4 %copy-start.2 = (bf16[512]{0:T(512)(128)(2,1)S(1)}, bf16[512]{0:T(512)(128)(2,1)}, u32[]{:S(2)}) copy-start(bf16[512]{0:T(512)(128)(2,1)} %param.28) | copy-start | bytes 3076
  181.3 105.1 %all-gather.14.cloned.1.call-start = ((), (), s32[]{:S(2)}) async-start(), calls=%async_computation.3 | async-start | bytes 2228224 | tf_op jit(solution)/shard_map/all_gather | solution.py:45
  193.0 171.1 %all-gather.16.cloned.1.call-start = ((), (), s32[]{:S(2)}) async-start(), calls=%async_computation.4 | async-start | bytes 4456448 | tf_op jit(solution)/shard_map/all_gather | solution.py:29
  220.7 213.9 %all-gather.18.cloned.1.call-start = ((), (), s32[]{:S(2)}) async-start(), calls=%async_computation.5 | async-start | bytes 2228224 | tf_op jit(solution)/shard_map/all_gather | solution.py:87
Sparse Core Ops, SparseCore 0:
  10.3 146.7 all-gather.11
  181.4 37.1 all-gather.19
  220.7 65.6 all-gather.13
  288.4 75.5 all-gather.15
  365.9 68.5 all-gather.17
where the time goes:
time: 481 us; the launch traced here: 480 us
  waiting for transfers between devices  307 us (64%)
  blocking collectives  119 us (25%)
  matrix products  22.6 us (5%)
  between operations  14.2 us (3%)
  other arithmetic  8.16 us (2%)
  local copies, waits for them, and re-layouts  7.16 us (1%)
    all_gather x1, waiting for transfers between devices, sent_together(): out = lax.all_gather(both, axis, axis=dim, tiled=True)  142 us
    all_gather x2, waiting for transfers between devices, entering_2(): pieces = jax.tree.map(lambda part: lax.all_gather(part, axis), total)  93 us
    all_gather x1, waiting for transfers between devices, whole_of(): out = lax.all_gather(out, axes[number], axis=dim, tiled=True)  65.2 us
    all_gather x2, blocking collectives, prefix_by_axis(): lax.all_gather(part.astype(kind), axis)  34.3 us
    all_to_all x1, blocking collectives, sent_and_summed(): parts = lax.all_to_all(in_blocks(x, dim, length), axis, 0, 0, tiled=True)  23.2 us
    all_gather x1, blocking collectives, entering_2(): pieces = jax.tree.map(lambda part: lax.all_gather(part, axis), total)  21.9 us
    unnamed x2, blocking collectives  16.9 us
    all_to_all x1, blocking collectives, copy_for_each(): return lax.all_to_all(copies, axis, split_axis=0, concat_axis=0, tiled=True)  12.8 us
  transfers between devices with their start and end apart: 7, of which 5 were waited for; matrix products, arithmetic and copies ran while one was open for 5% of the time, Pallas kernels for 0%

commit v1 on v0

v1 whole, which is shorter than its diff:
```python
import functools

import jax
import jax.numpy as jnp
from jax import lax
from jax.experimental import pallas as pl
from jax.experimental.pallas import tpu as pltpu
from jax.sharding import Mesh
from jax.sharding import PartitionSpec as P

MESH = pl.DeviceIdType.MESH
F32 = jnp.float32
BF16 = jnp.bfloat16
EPS = 1e-05
L = 128
HD = 64
KERNEL = 5
SP = ("z", "y")
TP = ("x", "c")


def dot(a, b):
    return jnp.dot(a, b, preferred_element_type=F32)


def dot_nt(a, b):
    return lax.dot_general(a, b, (((1,), (1,)), ((), ())), preferred_element_type=F32)


def iota(shape, dim):
    return lax.broadcasted_iota(jnp.int32, shape, dim)


def send(src, dst, ss, rs, dev):
    return pltpu.make_async_remote_copy(
        src_ref=src, dst_ref=dst, send_sem=ss, recv_sem=rs, device_id=dev, device_id_type=MESH
    )


def silu(x):
    return x / (1.0 + jnp.exp(-x))


def softplus(x):
    return jnp.maximum(x, 0.0) + jnp.log1p(jnp.exp(-jnp.abs(x)))


def kernel(dims, *refs):
    Z, Y, X, C, D, DR = dims
    (tok, gain, wv, wg, wk, wr, wsf, wsb, wo, cv, ck, cr, bias, rate, ngain,
     out,
     slab, normed, hs, hr, w1, wfull, wot, rawp, krs, krall, kmat, rmat, ktr, vals,
     cfin, cT, sT, ecar, tots, totr, sst, srv, hf, hb, hst, hrv, yw, ast, arv,
     pbuf, prv, qbuf, xrv,
     s1_s, s1_r, tk_s, tk_r, rg_s, rg_r, hl_s, hl_r, kr_s, kr_r, tt_s, tt_r, ss_s, ss_r,
     hh_s, hh_r, aa_s, aa_r, wy_s, wy_r, dp_s, dp_r, xr_s, xr_r, xg_s, xg_r, dg_s, dg_r) = refs
    T = Y * L
    DH = D // C
    NS = L // Z
    PR = L // (X * C)
    z, y, x, c = (lax.axis_index(a) for a in ("z", "y", "x", "c"))
    up = lambda i, n, k: lax.rem(i + k, n)
    dn = lambda i, n, k: lax.rem(i + n - k, n)
    zr, zl = up(z, Z, 1), dn(z, Z, 1)
    yr, yl, yo = up(y, Y, 1), dn(y, Y, 1), up(y, Y, 2)
    oc = 1 - c
    lane = iota((1, L), 1)
    sent = []

    def go(*a):
        copy = send(*a)
        copy.start()
        sent.append(copy)

    barrier = pltpu.get_barrier_semaphore()
    near = [{"y": up(y, Y, k)} for k in range(1, Y)] + [{"x": up(x, X, k)} for k in range(1, X)]
    near += [{"z": zr}] + ([{"z": zl}] if Z > 2 else []) + ([{"c": oc}] if C > 1 else [])
    for dev in near:
        pl.semaphore_signal(barrier, inc=1, device_id=dev, device_id_type=MESH)

    onef = (iota((8, L), 1) == iota((8, L), 0) + HD).astype(BF16)
    oneb = (iota((8, L), 1) == iota((8, L), 0) + HD + 8).astype(BF16)
    if wsf.shape[1] != 8:
        n = wsf.shape[1]
        onef = (iota((n, L), 1) == iota((n, L), 0) + HD).astype(BF16)
        oneb = (iota((n, L), 1) == iota((n, L), 0) + HD + 8).astype(BF16)
    steps = dot(wsf[...], onef) + dot(wsb[...], oneb)
    kf, rf = wk[...].astype(F32), wr[...].astype(F32)
    parts = (kf, pltpu.roll(kf, HD, 1), rf, pltpu.roll(rf, HD, 1))
    for j in range(Y):
        w1[j, :, 0:L] = wv[:, j * L : (j + 1) * L]
        w1[j, :, L : 2 * L] = wg[:, j * L : (j + 1) * L]
        w1[j, :, 2 * L :] = jnp.where(lane < HD, parts[j], steps).astype(BF16)
    wfull[z, y] = w1[y]
    eye = (iota((DR, DR), 0) == iota((DR, DR), 1)).astype(BF16)
    wot[z, y] = dot_nt(eye, wo[...]).astype(BF16)
    slab[y] = tok[...]
    pl.semaphore_wait(barrier, len(near))

    for k in range(1, Y):
        go(w1.at[up(y, Y, k)], wfull.at[z, y], s1_s.at[k], s1_r.at[k], {"y": up(y, Y, k)})
    cs = pl.ds(pl.multiple_of(c * DH, DH), DH)
    go(tok.at[:, cs], slab.at[y, :, cs], tk_s.at[0], tk_r.at[0], {"y": yr})
    go(tok.at[:, cs], slab.at[y, :, cs], tk_s.at[1], tk_r.at[1], {"y": yl})

    half = Z // 2

    def blk(k, zz):
        return wot.at[zz, y] if k == 4 else wfull.at[zz, dn(y, Y, k)]

    def count(d, k):
        return half if (d == 0) == (k in (0, 1, 4)) else half - 1

    def ring(s):
        for k in range(5):
            for d in (0, 1):
                zz = dn(z, Z, s) if d == 0 else up(z, Z, s)
                ref = blk(k, zz)
                dev = {"z": zr if d == 0 else zl}
                if s == 0:
                    if d == 0 and 0 < k < 4:
                        send(ref, ref, s1_s.at[k], s1_r.at[k], {"y": yr}).wait_recv()
                elif s - 1 < count(d, k):
                    send(ref, ref, rg_s.at[d, s - 1, k], rg_r.at[d, s - 1, k], dev).wait_recv()
                if s < count(d, k):
                    go(ref, ref, rg_s.at[d, s, k], rg_r.at[d, s, k], dev)

    def tokens_one():
        lo, hi = pl.ds(0, L // 2), pl.ds(L // 2, L // 2)
        ref = slab.at[yl, :, cs]
        send(ref, ref, tk_s.at[0], tk_r.at[0], {"y": yr}).wait_recv()
        go(slab.at[yl, lo, cs], slab.at[yl, lo, cs], tk_s.at[2], tk_r.at[2], {"y": yr})
        if C > 1:
            go(ref, ref, tk_s.at[4], tk_r.at[4], {"c": oc})
        ref = slab.at[yr, :, cs]
        send(ref, ref, tk_s.at[1], tk_r.at[1], {"y": yl}).wait_recv()
        go(slab.at[yr, hi, cs], slab.at[yr, hi, cs], tk_s.at[3], tk_r.at[3], {"y": yl})
        if C > 1:
            go(ref, ref, tk_s.at[5], tk_r.at[5], {"c": oc})

    def tokens_two():
        for i, rows in ((2, pl.ds(0, L // 2)), (3, pl.ds(L // 2, L // 2))):
            ref = slab.at[yo, rows, cs]
            send(ref, ref, tk_s.at[i], tk_r.at[i], {"y": yr}).wait_recv()
        if C > 1:
            ref = slab.at[yo, :, cs]
            go(ref, ref, tk_s.at[6], tk_r.at[6], {"c": oc})

    def tokens_three():
        if C > 1:
            co = pl.ds(pl.multiple_of(oc * DH, DH), DH)
            for i, b in ((4, yl), (5, yr), (6, yo)):
                ref = slab.at[b, :, co]
                send(ref, ref, tk_s.at[i], tk_r.at[i], {"c": oc}).wait_recv()
        hs[0] = slab[Y - 1, L - 16 :, :].astype(F32)[8:].astype(BF16)
        hs[1] = slab[0, 0:16, :].astype(F32)[:8].astype(BF16)
        go(hs.at[0], hr.at[0], hl_s.at[0], hl_r.at[0], {"z": zr})
        go(hs.at[1], hr.at[1], hl_s.at[1], hl_r.at[1], {"z": zl})

    def norm(v):
        v = v.astype(F32)
        return v * lax.rsqrt(jnp.mean(v * v, -1, keepdims=True) + EPS) * gain[...].astype(F32)

    def normalize():
        def tile(i, carry):
            r = pl.multiple_of(i * 32, 32)
            normed[pl.ds(r, 32), :] = norm(slab[lax.div(i, 4), pl.ds(lax.rem(i, 4) * 32, 32), :]).astype(BF16)
            return carry
        lax.fori_loop(0, T // 32, tile, 0)

    last = max(half - 1, 0)
    for s in range(half + 1):
        ring(s)
        if s == min(3, last):
            tokens_one()
        if s == min(5, last):
            tokens_two()
        if s == min(7, last):
            tokens_three()
            normalize()

    for i in (0, 1):
        send(hr.at[i], hr.at[i], hl_s.at[i], hl_r.at[i], {"z": zr}).wait_recv()
    go(wot.at[:, y], wot.at[:, y], wy_s.at[0], wy_r.at[0], {"y": yr})
    go(wot.at[:, y], wot.at[:, y], wy_s.at[1], wy_r.at[1], {"y": yl})

    hn = jnp.concatenate([norm(hr[0]), norm(hr[1])], axis=0).astype(BF16)
    w = wfull[...].reshape(D, 3 * L)
    rh = dot(hn, w).astype(BF16).astype(F32)
    rawp[0:8, :] = jnp.where(z > 0, rh[0:8], 0.0)
    rawp[T + 8 :, :] = jnp.where(z < Z - 1, rh[8:16], 0.0)

    def project(b, carry):
        r = pl.multiple_of(b * L, L)
        rawp[pl.ds(r + 8, L), :] = dot(normed[pl.ds(r, L), :], wfull[...].reshape(D, 3 * L)).astype(BF16).astype(F32)
        return carry
    lax.fori_loop(0, Y, project, 0)

    def conv(lo, taps):
        acc = rawp[6 : 6 + T, lo : lo + L] * taps[0:1]
        for k in range(1, KERNEL):
            acc = acc + rawp[6 + k : 6 + k + T, lo : lo + L] * taps[k : k + 1]
        return silu(acc).astype(BF16)

    taps = jnp.where(y < 2, ck[...].astype(F32), cr[...].astype(F32))
    taps = jnp.where(lax.rem(y, 2) == 1, pltpu.roll(taps, HD, 1), taps)
    kr = conv(2 * L, taps).astype(F32)
    krs[...] = jnp.where(lane < HD, kr[: T // 2], pltpu.roll(kr[T // 2 :], HD, 1)).astype(BF16)
    for k in range(1, Y):
        go(krs, krall.at[y], kr_s.at[k], kr_r.at[k], {"y": up(y, Y, k)})
    krall[y] = krs[...]

    pre = pltpu.roll(rawp[8 : 8 + T, 2 * L :], lax.rem(HD + L - 2 * y, L), 1)

    def row(ref):
        val = jnp.zeros((1, L), F32)
        for d in (0, 1):
            for h in (0, 1):
                val = jnp.where(lane == 8 * d + h, ref[d, 2 * y + h], val)
        return val
    step = softplus(pre + row(bias))
    ld = -row(rate) * step
    hi = ld.astype(BF16)
    rest = ld - hi.astype(F32)
    mid = rest.astype(BF16)
    low = (rest - mid.astype(F32)).astype(BF16)
    tri = (iota((T, T), 1) <= iota((T, T), 0)).astype(BF16)
    cum = dot(tri, hi) + dot(tri, mid) + dot(tri, low)
    tot = cum[T - 1 : T]
    cfin[...] = jnp.where(lane < 8, cum, tot - cum + ld)
    cT[...] = cfin[...].T
    sT[...] = step.T
    ecar[...] = jnp.exp(cfin[...])
    damp = jnp.exp(tot)

    def spread(m, l):
        return jnp.where(lane < HD, m[:, l : l + 1], m[:, l + 1 : l + 2])
    tots[...] = jnp.concatenate([jnp.broadcast_to(spread(damp, 0), (4, L)), jnp.broadcast_to(spread(damp, 8), (4, L))], axis=0)
    for k in range(1, Z):
        go(tots, totr.at[z], tt_s.at[k], tt_r.at[k], {"z": up(z, Z, k)})
    totr[z] = tots[...]

    wdec = jnp.exp(tot - cfin[...]) * step
    vals[...] = conv(0, cv[:, pl.ds(pl.multiple_of(y * L, L), L)].astype(F32))
    vf = vals[...].astype(F32)
    scaled = [(vf * spread(wdec, l)).astype(BF16) for l in (0, 8)]

    for k in range(1, Y):
        ref = krall.at[dn(y, Y, k)]
        send(krs, ref, kr_s.at[k], kr_r.at[k], {"y": yr}).wait_recv()
    for m, i in ((kmat, 0), (rmat, 2)):
        a, b = krall[i].astype(F32), krall[i + 1].astype(F32)
        m[0 : T // 2] = jnp.where(lane < HD, a, pltpu.roll(b, HD, 1)).astype(BF16)
        m[T // 2 :] = jnp.where(lane < HD, pltpu.roll(a, HD, 1), b).astype(BF16)
    ktr[...] = kmat[...].astype(F32).T.astype(BF16)
    sf, sb = dot(ktr[...], scaled[0]), dot(ktr[...], scaled[1])
    sst[...] = jnp.concatenate([sf.reshape(Z, NS, L), sb.reshape(Z, NS, L)], axis=1).astype(BF16)
    for k in range(1, Z):
        to = up(z, Z, k)
        go(sst.at[to], srv.at[z], ss_s.at[k], ss_r.at[k], {"z": to})
    srv[z] = sst[z]

    lo, hi = pl.ds(0, half), pl.ds(half, half)
    for i, b in ((0, yl), (1, yr)):
        ref = wot.at[:, b]
        send(ref, ref, wy_s.at[i], wy_r.at[i], {"y": yr}).wait_recv()
    go(wot.at[lo, yl], wot.at[lo, yl], wy_s.at[2], wy_r.at[2], {"y": yr})
    go(wot.at[hi, yr], wot.at[hi, yr], wy_s.at[3], wy_r.at[3], {"y": yl})

    def within(b, carry):
        r = pl.multiple_of(b * L, L)
        sc = dot(rmat[pl.ds(r, L), :], ktr[...])
        i, j = iota((L, T), 0) + r, iota((L, T), 1)
        ci = cfin[pl.ds(r, L), :]
        ys = []
        for h in (0, 1):
            gap = jnp.where(j <= i, ci[:, h : h + 1] - cT[h : h + 1, :], ci[:, 8 + h : 9 + h] - cT[8 + h : 9 + h, :])
            fw, bw = sT[h : h + 1, :], sT[8 + h : 9 + h, :]
            weight = jnp.where(j < i, fw, jnp.where(j > i, bw, fw + bw))
            ys.append(dot((sc * jnp.exp(gap) * weight).astype(BF16), vals[...]))
        yw[pl.ds(r, L), :] = jnp.where(lane < HD, ys[0], ys[1])
        return carry
    lax.fori_loop(0, Y, within, 0)

    for k in range(1, Z):
        fr = dn(z, Z, k)
        send(tots, totr.at[fr], tt_s.at[k], tt_r.at[k], {"z": fr}).wait_recv()
        send(sst.at[fr], srv.at[fr], ss_s.at[k], ss_r.at[k], {"z": fr}).wait_recv()
    h = jnp.zeros((NS, L), F32)
    for k in range(Z):
        hf[k] = h
        h = totr[k, 0:1] * h + srv[k].astype(F32)[:NS]
    h = jnp.zeros((NS, L), F32)
    for k in reversed(range(Z)):
        hb[k] = h
        h = totr[k, 4:5] * h + srv[k].astype(F32)[NS:]
    hst[...] = jnp.concatenate([hf[...], hb[...]], axis=1).astype(BF16)
    for k in range(1, Z):
        to = up(z, Z, k)
        go(hst.at[to], hrv.at[z], hh_s.at[k], hh_r.at[k], {"z": to})
    hrv[z] = hst[z]
    for k in range(1, Z):
        fr = dn(z, Z, k)
        send(hst.at[fr], hrv.at[fr], hh_s.at[k], hh_r.at[k], {"z": fr}).wait_recv()
    hm = hrv[...].astype(F32)
    hfm = hm[:, :NS].reshape(L, L).astype(BF16)
    hbm = hm[:, NS:].reshape(L, L).astype(BF16)

    cols = pl.ds(pl.multiple_of(y * L, L), L)
    ng = ngain[:, cols].astype(F32)

    def finish(b, carry):
        r = pl.multiple_of(b * L, L)
        rm = rmat[pl.ds(r, L), :]
        e = ecar[pl.ds(r, L), :]
        yy = yw[pl.ds(r, L), :] + spread(e, 0) * dot(rm, hfm) + spread(e, 8) * dot(rm, hbm)
        g = yy * silu(rawp[pl.ds(r + 8, L), L : 2 * L])
        sq = g * g
        m0 = jnp.sum(jnp.where(lane < HD, sq, 0.0), -1, keepdims=True)
        m1 = jnp.sum(jnp.where(lane < HD, 0.0, sq), -1, keepdims=True)
        ms = jnp.where(lane < HD, m0, m1) * (1.0 / HD)
        ast[b] = (g * lax.rsqrt(ms + EPS) * ng).astype(BF16)
        return carry
    lax.fori_loop(0, Y, finish, 0)
    for k in range(1, Y):
        to = up(y, Y, k)
        go(ast.at[to], arv.at[y], aa_s.at[k], aa_r.at[k], {"y": to})
    arv[y] = ast[y]

    for i, rows, b in ((2, lo, yo), (3, hi, yo)):
        ref = wot.at[rows, b]
        send(ref, ref, wy_s.at[i], wy_r.at[i], {"y": yr}).wait_recv()
    for k in range(1, Y):
        fr = dn(y, Y, k)
        send(ast.at[fr], arv.at[fr], aa_s.at[k], aa_r.at[k], {"y": fr}).wait_recv()

    a = jnp.concatenate([arv[k] for k in range(Y)], axis=1)
    zg = min(Z, 4)
    wide = zg * Y * DR

    def part(t, carry):
        wt = wot[pl.ds(t * zg, zg)].reshape(wide, Y * L)
        pbuf[:, pl.ds(pl.multiple_of(t * wide, wide), wide)] = dot_nt(a, wt).astype(BF16)
        return carry
    lax.fori_loop(0, Z // zg, part, 0)

    HR = L // C
    mine = pl.ds(pl.multiple_of(c * HR, HR), HR)
    if C > 1:
        other = pl.ds(pl.multiple_of(oc * HR, HR), HR)
        go(pbuf.at[other], prv, dp_s.at[0], dp_r.at[0], {"c": oc})
        send(prv, prv, dp_s.at[0], dp_r.at[0], {"c": oc}).wait_recv()
        qbuf[...] = (pbuf[mine, :].astype(F32) + prv[...].astype(F32)).astype(BF16).reshape(X, PR, D)
    else:
        qbuf[...] = pbuf[...].reshape(X, PR, D)
    for k in range(1, X):
        to = up(x, X, k)
        go(qbuf.at[to], xrv.at[k], xr_s.at[k], xr_r.at[k], {"x": to})
    total = qbuf[x].astype(F32)
    for k in range(1, X):
        send(xrv.at[k], xrv.at[k], xr_s.at[k], xr_r.at[k], {"x": x}).wait_recv()
        total = total + xrv[k].astype(F32)

    def rows_of(xx, cc):
        return out.at[pl.ds(pl.multiple_of(cc * HR + xx * PR, PR), PR)]
    own = rows_of(x, c)
    own[...] = total.astype(BF16)
    for k in range(1, X):
        go(own, own, xg_s.at[k], xg_r.at[k], {"x": up(x, X, k)})
    if C > 1:
        go(own, own, dg_s.at[0], dg_r.at[0], {"c": oc})
    for k in range(1, X):
        ref = rows_of(dn(x, X, k), c)
        send(ref, ref, xg_s.at[k], xg_r.at[k], {"x": x}).wait_recv()
        if C > 1:
            go(ref, ref, dg_s.at[k], dg_r.at[k], {"c": oc})
    if C > 1:
        for k in range(X):
            ref = rows_of(dn(x, X, k), oc)
            send(ref, ref, dg_s.at[k], dg_r.at[k], {"c": oc}).wait_recv()
    for copy in sent:
        copy.wait_send()


def body(dims, *args):
    Z, Y, X, C, D, DR = dims
    T, NS = Y * L, L // Z
    PR = L // (X * C)
    half = max(Z // 2, 1)
    dma = pltpu.SemaphoreType.DMA
    vm = pltpu.VMEM
    in_args = list(args)
    in_args[1] = args[1].reshape(1, -1)
    in_args[13] = args[13].reshape(1, -1)
    order = in_args[:8] + [in_args[14]] + in_args[8:14]
    spaces = [pltpu.VMEM] * 12 + [pltpu.SMEM] * 2 + [pltpu.VMEM]
    scratch = [
        vm((Y, L, D), BF16),
        vm((T, D), BF16),
        vm((2, 8, D), BF16),
        vm((2, 8, D), BF16),
        vm((Y, DR, 3 * L), BF16),
        vm((Z, Y, DR, 3 * L), BF16),
        vm((Z, Y, DR, Y * L), BF16),
        vm((T + 16, 3 * L), F32),
        vm((T // 2, L), BF16),
        vm((Y, T // 2, L), BF16),
        vm((T, L), BF16),
        vm((T, L), BF16),
        vm((L, T), BF16),
        vm((T, L), BF16),
        vm((T, L), F32),
        vm((L, T), F32),
        vm((L, T), F32),
        vm((T, L), F32),
        vm((8, L), F32),
        vm((Z, 8, L), F32),
        vm((Z, 2 * NS, L), BF16),
        vm((Z, 2 * NS, L), BF16),
        vm((Z, NS, L), F32),
        vm((Z, NS, L), F32),
        vm((Z, 2 * NS, L), BF16),
        vm((Z, 2 * NS, L), BF16),
        vm((T, L), F32),
        vm((Y, L, L), BF16),
        vm((Y, L, L), BF16),
        vm((L, D), BF16),
        vm((L // C, D), BF16),
        vm((X, PR, D), BF16),
        vm((X, PR, D), BF16),
    ]
    for shape in ((Y,), (7,), (2, half, 5), (2,), (Y,), (Z,), (Z,), (Z,), (Y,), (4,), (1,), (X,), (X,), (X,)):
        scratch += [dma(shape), dma(shape)]
    return pl.pallas_call(
        functools.partial(kernel, dims),
        out_shape=jax.ShapeDtypeStruct((L, D), BF16),
        in_specs=[pl.BlockSpec(memory_space=s) for s in spaces],
        out_specs=pl.BlockSpec(memory_space=pltpu.VMEM),
        scratch_shapes=scratch,
        compiler_params=pltpu.CompilerParams(
            collective_id=0, has_side_effects=True, vmem_limit_bytes=60 * 2**20
        ),
    )(*order)


def build(mesh, Z, Y, X, C, D):
    split = Mesh(mesh.devices.reshape(Z, Y, X, C), SP + TP)
    dims = (Z, Y, X, C, D, D // (Z * Y))
    both = P(SP, TP)
    in_specs = (
        P(SP, None), P(), both, both, both, both, both, both,
        P(None, TP), P(None, TP), P(None, TP), P(None, TP), P(None, TP), P(TP), P(TP, SP),
    )
    return jax.shard_map(
        functools.partial(body, dims), mesh=split, in_specs=in_specs, out_specs=P(SP, None), check_vma=False
    )


def solution(mesh):
    return build(mesh, 16, 4, 4, 2, 2048)
```

time: 481 us -> 109 us (0.23)
  waiting for transfers between devices: 307 us -> 0 us
  blocking collectives: 119 us -> 0 us
  Pallas kernels: 0 us -> 101 us
  matrix products: 22.6 us -> 0 us
  between operations: 14.2 us -> 0.01 us
  other arithmetic: 8.16 us -> 0 us
    all_gather x5 -> x0, waiting for transfers between devices: 306 us -> none  [the longest x1 142 us: sent_together(): out = lax.all_gather(both, axis, axis=dim, tiled=True)]
    pallas_call x0 -> x1, Pallas kernels: none -> 101 us  [body(): pl.pallas_call(functools.partial(kernel, dims), out_shape=jax.ShapeDtypeS...]
    all_gather x4 -> x0, blocking collectives: 66.1 us -> none  [the longest x2 34.3 us: prefix_by_axis(): lax.all_gather(part.astype(kind), axis)]
    all_to_all x2 -> x0, blocking collectives: 36 us -> none  [the longest x1 23.2 us: sent_and_summed(): parts = lax.all_to_all(in_blocks(x, dim, length), axis, 0, 0, tiled=True)]
    dot_general x15 -> x0, matrix products: 22.6 us -> none  [the longest x6 10.6 us: body(): jnp.dot(normed, weight, preferred_element_type=jnp.float32)]
    unnamed x2 -> x0, blocking collectives: 16.9 us -> none
  transfers between devices with their start and end apart: 7 -> 0, of which waited for: 5 -> 0; matrix products, arithmetic and copies ran while one was open for 5% -> 0% of each run, Pallas kernels for 0% -> 0%
where the time goes in v1:
time: 109 us
  Pallas kernels  101 us (93%)
  local copies, waits for them, and re-layouts  7.91 us (7%)
    pallas_call x1, Pallas kernels, body(): pl.pallas_call(functools.partial(kernel, dims), out_shape=jax.ShapeDtypeS...  101 us
    unnamed x6, local copies, waits for them, and re-layouts  5.34 us

profile of v1, /device:TPU:1, one launch (start us, length us, event | category | flops | bytes accessed | tf_op | source)
XLA Modules:
  0.0 108.8 jit_solution(1675693504666128759)
XLA Ops:
  0.0 0.0 copy-start
  0.0 1.3 %reshape.7.refs_14_ = bf16[1,512]{1,0:T(2,128)(2,1)} reshape(bf16[512]{0:T(512)(128)(2,1)} %param.28) | data formatting | bytes 2048 | tf_op jit(solution)/shard_map/reshape | solution.py:394
  1.3 1.3 %reshape.6.refs_1_ = bf16[1,2048]{1,0:T(2,128)(2,1)} reshape(bf16[2048]{0:T(1024)(128)(2,1)} %param.16) | data formatting | bytes 8192 | tf_op jit(solution)/shard_map/reshape | solution.py:393
  2.6 1.4 %copy.16.refs_6_ = bf16[32,8]{1,0:T(8,128)(2,1)} copy(bf16[32,8]{0,1:T(8,128)(2,1)} %param.21) | data formatting | bytes 1024 | tf_op args[6]
  3.9 1.3 %copy.17.refs_7_ = bf16[32,8]{1,0:T(8,128)(2,1)} copy(bf16[32,8]{0,1:T(8,128)(2,1)} %param.22) | data formatting | bytes 1024 | tf_op args[7]
  5.3 0.0 copy-done
  5.3 0.8 copy.18.refs_8_
  6.0 100.9 %shard_map.145 = bf16[128,2048]{1,0:T(8,128)(2,1)} custom-call(bf16[128,2048]{1,0:T(8,128)(2,1)} %refs_0_.1, bf16[1,2048]{1,0:T(2,128)(2,1)} %reshape.6.refs_1_, bf16[32,512]{1,0:T(8,128)(2,1)} %refs_2_.1, bf16[32,512]{1,0:T(8,128)(2,1)} %refs_3_.1, bf16[32,128]{1,0:T(8,128)(2,1)} %refs_4_.1, bf16[32,128]{1,0:T(8,128)(2,1)} %refs_5_.1, ...), custom_call_target="tpu_custom_call" | custom-call | tf_op jit(solution)/shard_map/pallas_call | solution.py:434
  106.9 1.9 %copy.20 = bf16[128,2048]{1,0:T(8,128)(2,1)} copy(bf16[128,2048]{1,0:T(8,128)(2,1)} %shard_map.145) | data formatting | bytes 1048576
Async XLA Ops:
  0.0 5.3 %copy-start = (bf16[512,32]{0,1:T(8,128)(2,1)S(1)}, bf16[512,32]{0,1:T(8,128)(2,1)}, u32[]{:S(2)}) copy-start(bf16[512,32]{0,1:T(8,128)(2,1)} %param.29) | copy-start | bytes 98308
